TPU v7x, 256 devices: a 4x2x16 block of a 4x16x16 slice. The times are simulated.
256 devices in a mesh: grp: 2 (over y), sp: 32 (over z, core), tp: 4 (over x).
Axes of the slice: x: 4, y: 2, z: 16, core: 2. Of those that a mesh axis runs over, the one named last changes fastest.
The devices are a block of a 4x16x16 slice.
Arguments:
- stream_in: bfloat16 [32768, 2048], P(('grp', 'sp')), parts along dimension 0, may hold values from -6 to 6
- query_wide: bfloat16 [32768, 1024], P(('grp', 'sp'), 'tp'), parts along dimension 0, may hold values from -6 to 6
- key_wide: bfloat16 [32768, 1024], P(('grp', 'sp'), 'tp'), parts along dimension 0, may hold values from -6 to 6
- value_wide: bfloat16 [32768, 2048], P(('grp', 'sp'), 'tp'), parts along dimension 0, may hold values from -6 to 6
- query_narrow: bfloat16 [32768, 512], P(('grp', 'sp'), 'tp'), parts along dimension 0, may hold values from -6 to 6
- key_narrow: bfloat16 [32768, 512], P(('grp', 'sp'), 'tp'), parts along dimension 0, may hold values from -6 to 6
- value_narrow: bfloat16 [32768, 1024], P(('grp', 'sp'), 'tp'), parts along dimension 0, may hold values from -6 to 6
- decay_wide: float32 [4, 32768], P('tp', ('grp', 'sp')), parts along dimension 1, may hold values from -1 to 0
- decay_narrow: float32 [4, 32768], P('tp', ('grp', 'sp')), parts along dimension 1, may hold values from -1 to 0
- gain_wide: float32 [2048], P('tp'), may hold values from 0.1 to 1.9
- gain_narrow: float32 [1024], P('tp'), may hold values from 0.1 to 1.9
- out_wide: bfloat16 [2048, 2048], P('tp'), may hold values from -0.109375 to 0.109375
- out_narrow: bfloat16 [1024, 2048], P('tp'), may hold values from -0.109375 to 0.109375
- mlp_gain: float32 [2048], replicated, may hold values from 0.1 to 1.9
- up_weight: bfloat16 [2048, 8192], P('sp', 'tp'), may hold values from -0.125 to 0.125
- down_weight: bfloat16 [8192, 2048], P('tp', 'sp'), may hold values from -0.0625 to 0.0625
Outputs:
- stream_out: bfloat16 [32768, 2048], P(('grp', 'sp', 'tp')), parts along dimension 0
There are 2 independent parts, one for each index of `grp`. A program takes and returns all parts, laid end to end along the dimension named above; an argument that names none is the same for every part. Nothing has to cross between parts.
All inputs are finite; a program needn't handle non-finite values.
Results may differ from a plain program's by a relative error of at most 0.019.
Values may be sent and summed in bfloat16 or wider, within the bound.
No kernel may reach another device: no remote copies, remote signals or barrier semaphores. Data moves between devices by JAX's collectives and lax.ppermute only.
A program may use at most 128 MiB of HBM per device.

v0:
```python
import jax
import jax.numpy as jnp
from jax import lax
from jax.sharding import Mesh
from jax.sharding import PartitionSpec as P

SP = ("sp_0", "sp_1")
GRP_SP = ("grp", "sp_0", "sp_1")
GRP_SP_TP = ("grp", "sp_0", "sp_1", "tp")
EPS = 1e-06


def neutral_like(x, identity):
    return jax.tree.map(
        lambda a, e: jnp.broadcast_to(jnp.asarray(e, a.dtype), a.shape), x, identity
    )


def entering(x, axes, combine, identity):
    before = start = neutral_like(x, identity)
    total = x
    for axis in reversed(axes):
        length, mine = (lax.axis_size(axis), lax.axis_index(axis))
        pieces = jax.tree.map(
            lambda part, kind: lax.all_gather(part.astype(kind), axis),
            total,
            (jnp.bfloat16, jnp.bfloat16, jnp.bfloat16, jnp.bfloat16),
        )
        inside, total = (start, start)
        for k in range(length):
            passed = k < mine
            total = combine(
                total, jax.tree.map(lambda part, own: part[k].astype(own.dtype), pieces, x)
            )
            inside = jax.tree.map(lambda new, old: jnp.where(passed, new, old), total, inside)
        before = combine(inside, before)
    return before


def rows_first(arrays, axis, dims):
    turned = [jnp.moveaxis(a, dim, 0) for a, dim in zip(arrays, dims)]
    both = jnp.concatenate([t.reshape(len(t), -1) for t in turned], axis=1)
    result, at, done = (lax.all_gather(both, axis, axis=0, tiled=True), 0, [])
    for t, dim in zip(turned, dims):
        slab = result[:, at : at + t[0].size].reshape(-1, *t.shape[1:])
        done.append(jnp.moveaxis(slab, 0, dim))
        at += t[0].size
    return tuple(done)


def split_up(x, dim, length):
    before, after = (x.shape[:dim], x.shape[dim + 1 :])
    return jnp.moveaxis(x.reshape(*before, length, -1, *after), dim, 0)


def summed_on_arrival(x, axis, dim):
    parts = split_up(x, dim, lax.axis_size(axis))
    arrived = lax.all_to_all(parts, axis, split_axis=0, concat_axis=0, tiled=True)
    return arrived.astype(jnp.float32).sum(axis=0)


def joined_along(parts, dim):
    parts = jnp.moveaxis(parts, 0, dim)
    lengths = parts.shape
    return parts.reshape(*lengths[:dim], lengths[dim] * lengths[dim + 1], *lengths[dim + 2 :])


def copy_for_each(x, axis):
    length = lax.axis_size(axis)
    return lax.all_to_all(jnp.broadcast_to(x[None], (length, *x.shape)), axis, 0, 0, tiled=True)


def collect(x, axis, dim):
    return joined_along(copy_for_each(x, axis), dim)


def retain_local(queries, key_rows, value_rows, log_decay):
    total_heads = log_decay.shape[0]
    length = queries.shape[0]
    key_width = queries.shape[1] // total_heads
    value_width = value_rows.shape[1] // total_heads
    query_heads = queries.reshape(length, total_heads, key_width)
    key_heads = key_rows.reshape(length, total_heads, key_width)
    value_heads = value_rows.reshape(length, total_heads, value_width)
    cumulative = jnp.cumsum(log_decay, axis=1)
    row_index = lax.broadcasted_iota(jnp.int32, (length, length), 0)
    col_index = lax.broadcasted_iota(jnp.int32, (length, length), 1)
    causal = (row_index >= col_index)[None]
    log_gap = cumulative[:, :, None] - cumulative[:, None, :]
    fading = jnp.where(causal, jnp.exp(jnp.where(causal, log_gap, 0.0)), 0.0)
    scores = jnp.einsum("ihd,jhd->hij", query_heads, key_heads, preferred_element_type=jnp.float32)
    weights_low = (scores * key_width ** (-0.5) * fading).astype(jnp.bfloat16)
    within = jnp.einsum(
        "hij,jhe->ihe", weights_low, value_heads, preferred_element_type=jnp.float32
    )
    to_end = jnp.exp(cumulative[:, -1:] - cumulative)
    keyed = (key_heads.astype(jnp.float32) * key_width ** (-0.5) * to_end.T[:, :, None]).astype(
        jnp.bfloat16
    )
    local_state = jnp.einsum("jhd,jhe->hde", keyed, value_heads, preferred_element_type=jnp.float32)
    overall = jnp.exp(cumulative[:, -1])
    return (query_heads, cumulative, within, overall, local_state)


def finish(query_heads, cumulative, within, incoming, gain_values):
    carried = (
        jnp.einsum(
            "ihd,hde->ihe",
            query_heads.astype(jnp.float32),
            incoming,
            precision=lax.Precision.HIGHEST,
        )
        * jnp.exp(cumulative).T[:, :, None]
    )
    retained = within + carried
    centered = retained - jnp.mean(retained, axis=-1, keepdims=True)
    scaled = centered * lax.rsqrt(jnp.mean(centered * centered, axis=-1, keepdims=True) + EPS)
    return (scaled.reshape(retained.shape[0], -1) * gain_values).astype(jnp.bfloat16)


def normalize(rows, gain_values):
    values = rows.astype(jnp.float32)
    scaled = values * lax.rsqrt(jnp.mean(values * values, axis=-1, keepdims=True) + EPS)
    return (scaled * gain_values).astype(jnp.bfloat16)


def join_states(earlier, latter):
    return (
        earlier[0] * latter[0],
        latter[0][:, None, None] * earlier[1] + latter[1],
        earlier[2] * latter[2],
        latter[2][:, None, None] * earlier[3] + latter[3],
    )


def on_device(
    stream_in,
    query_wide,
    key_wide,
    value_wide,
    query_narrow,
    key_narrow,
    value_narrow,
    decay_wide,
    decay_narrow,
    gain_wide,
    gain_narrow,
    out_wide,
    out_narrow,
    mlp_gain,
    up_weight,
    down_weight,
):
    length = stream_in.shape[0]
    portion = length // lax.axis_size("tp")
    member = lax.axis_index("tp")
    wide_query, wide_cum, wide_within, wide_factor, wide_state = retain_local(
        query_wide, key_wide, value_wide, decay_wide
    )
    thin_query, thin_cum, thin_within, thin_factor, thin_state = retain_local(
        query_narrow, key_narrow, value_narrow, decay_narrow
    )
    identity = (
        jnp.ones_like(wide_factor),
        jnp.zeros_like(wide_state),
        jnp.ones_like(thin_factor),
        jnp.zeros_like(thin_state),
    )
    incoming = entering(
        (wide_factor, wide_state, thin_factor, thin_state), SP, join_states, identity
    )
    normed_wide = finish(wide_query, wide_cum, wide_within, incoming[1], gain_wide)
    normed_thin = finish(thin_query, thin_cum, thin_within, incoming[3], gain_narrow)
    up_full, down_full = rows_first((up_weight, down_weight), SP, (0, 1))
    mixed_heads = summed_on_arrival(
        (
            jnp.dot(normed_wide, out_wide, preferred_element_type=jnp.float32)
            + jnp.dot(normed_thin, out_narrow, preferred_element_type=jnp.float32)
        ).astype(jnp.bfloat16),
        "tp",
        0,
    )
    own_stream = lax.dynamic_slice_in_dim(stream_in, member * portion, portion, 0)
    middle = (own_stream.astype(jnp.float32) + mixed_heads).astype(jnp.bfloat16)
    raised = jax.nn.relu(
        jnp.dot(
            collect(normalize(middle, mlp_gain), "tp", 0),
            up_full,
            preferred_element_type=jnp.float32,
        )
    )
    hidden = (raised * raised).astype(jnp.bfloat16)
    channel = summed_on_arrival(
        jnp.dot(hidden, down_full, preferred_element_type=jnp.float32).astype(jnp.bfloat16), "tp", 0
    )
    return (middle.astype(jnp.float32) + channel).astype(jnp.bfloat16)


def solution(mesh):
    torus = Mesh(
        mesh.devices.reshape(mesh.shape["grp"], 16, 2, mesh.shape["tp"]),
        ("grp", "sp_0", "sp_1", "tp"),
    )
    placed = (
        P(GRP_SP, None),
        P(GRP_SP, "tp"),
        P(GRP_SP, "tp"),
        P(GRP_SP, "tp"),
        P(GRP_SP, "tp"),
        P(GRP_SP, "tp"),
        P(GRP_SP, "tp"),
        P("tp", GRP_SP),
        P("tp", GRP_SP),
        P("tp"),
        P("tp"),
        P("tp", None),
        P("tp", None),
        P(),
        P(SP, "tp"),
        P("tp", SP),
    )
    return jax.shard_map(
        on_device, mesh=torus, in_specs=placed, out_specs=P(GRP_SP_TP, None), check_vma=False
    )
```

profile of v0, /device:TPU:33, one launch (start us, length us, event | category | flops | bytes accessed | tf_op | source)
XLA Modules:
  0.0 342.9 jit_solution(9512883190763255492)
XLA Ops:
  6.6 1.1 reduce-window.14
  7.8 0.2 slice_reduce_fusion.1
  7.9 0.2 reduce-window.15
  8.2 0.7 slice.363
  8.9 0.6 slice.362
  10.8 1.0 reduce-window.16
  11.8 0.2 slice_reduce_fusion
  12.2 0.6 slice.383
  12.8 0.6 slice.382
  14.7 1.3 dynamic-slice
  16.0 0.8 dynamic-update-slice
  16.7 0.8 dynamic-update-slice.2
  17.5 1.4 convolution_convert_fusion.1
  18.9 22.0 %all-gather.3 = bf16[256,256]{1,0:T(8,128)(2,1)S(1)} all-gather(bf16[128,256]{1,0:T(8,128)(2,1)S(1)} %convolution_convert_fusion.1), channel_id=5, replica_groups=mesh['grp'=2,'sp_0'=16,'sp_1'=2,'tp'=4] {'sp_1'}, dimensions={0}, use_global_device_ids=true | all-gather | bytes 196608 | tf_op jit(solution)/shard_map/all_gather | solution.py:25
  40.9 2.5 all-reduce.5
  43.4 0.6 slice_convert_fusion.1
  44.6 1.3 fusion.248
  46.7 1.5 convolution_convert_fusion
  48.3 2.2 all-gather.1
  50.5 1.4 fusion.115
  52.1 0.8 pad_maximum_fusion
  53.0 1.3 dynamic-slice.1
  54.3 0.7 fusion.317
  54.9 1.3 dynamic-update-slice.1
  56.3 1.3 dynamic-update-slice.3
  57.6 24.1 %all-reduce.4 = (bf16[16]{0:T(256)(128)(2,1)S(1)}, bf16[16]{0:T(256)(128)(2,1)S(1)}) all-reduce(bf16[16]{0:T(256)(128)(2,1)S(1)} %dynamic-update-slice.1, bf16[16]{0:T(256)(128)(2,1)S(1)} %dynamic-update-slice.3), channel_id=2, replica_groups=mesh['grp'=2,'sp_0'=16,'sp_1'=2,'tp'=4] {'sp_0'}, use_global_device_ids=true, to_apply=%add.1 | all-reduce | flops 32 | bytes 128
  82.9 0.7 fusion.315
  93.6 0.7 fusion.316
  105.6 2.3 fusion.18
  107.9 3.0 convolution_bitcast_fusion.1
  111.0 3.0 fusion.319
  114.2 2.8 fusion.116
  117.0 58.9 %all-gather.8.cloned.1.call-done = bf16[16,1,256,512]{3,2,1,0:T(8,128)(2,1)} async-done(((bf16[1,1,256,512]{3,2,1,0:T(8,128)(2,1)}), bf16[16,1,256,512]{3,2,1,0:T(8,128)(2,1)}) %all-gather.8.cloned.1.call-update) | async-done | bytes 4194320 | tf_op jit(solution)/shard_map/all_gather | solution.py:25
  175.9 6.0 %fusion.320 = (f32[512]{0:T(512)S(1)}, f32[1,512,512]{2,1,0:T(8,128)S(1)}) fusion(f32[1,512,512]{2,1,0:T(8,128)} %convolution_bitcast_fusion.1, f32[512]{0:T(512)S(1)} %exp.55, bf16[512,256]{1,0:T(8,128)(2,1)S(1)} %copy-done.9, bf16[16,1,256,512]{3,2,1,0:T(8,128)(2,1)} %all-gather.8.cloned.1.call-done, f32[]{:T(128)} %bitcast.30, f32[]{:T(128)} %bitcast.31, ...), kind=kOutput, calls=%fused_computation.358 | convolution fusion | flops 815529472 | bytes 7082078 | tf_op jit(solution)/shard_map/ihd,hde->ihe/dot_general | solution.py:107
  181.8 0.2 multiply_reduce_fusion
  182.1 2.8 add_convert_fusion
  184.9 4.7 %all-to-all-start = ((bf16[4,128,2048]{2,1,0:T(8,128)(2,1)}), bf16[4,128,2048]{2,1,0:T(8,128)(2,1)}, u32[]{:S(2)}, u32[]{:S(2)}) async-start(bf16[4,128,2048]{2,1,0:T(8,128)(2,1)} %bitcast.179), calls=%async_computation | async-start | bytes 4194304 | tf_op jit(solution)/shard_map/all_to_all | solution.py:58
  189.5 16.5 %all-to-all-done = bf16[4,128,2048]{2,1,0:T(8,128)(2,1)} async-done(((bf16[4,128,2048]{2,1,0:T(8,128)(2,1)}), bf16[4,128,2048]{2,1,0:T(8,128)(2,1)}, u32[]{:S(2)}, u32[]{:S(2)}) %all-to-all-start) | async-done | bytes 2097184 | tf_op jit(solution)/shard_map/all_to_all | solution.py:58
  206.0 2.1 convert_reduce_fusion.1
  208.1 1.4 fusion.21
  209.5 0.2 fusion.23
  209.7 0.2 broadcast_in_dim.16
  209.9 18.6 %all_to_all.15 = bf16[4,128,2048]{2,1,0:T(8,128)(2,1)} all-to-all(bf16[4,128,2048]{2,1,0:T(8,128)(2,1)S(1)} %broadcast_in_dim.16), channel_id=1, replica_groups=mesh['grp'=2,'sp_0'=16,'sp_1'=2,'tp'=4] {'tp'}, dimensions={0} | all-to-all | bytes 4194304 | tf_op jit(solution)/shard_map/all_to_all | solution.py:70
  228.5 60.1 %all-gather.12.cloned.1.call-done = bf16[2048,4096]{1,0:T(8,128)(2,1)} async-done(((bf16[64,4096]{1,0:T(8,128)(2,1)}), bf16[2048,4096]{1,0:T(8,128)(2,1)}) %all-gather.12.cloned.1.call-update) | async-done | bytes 16777232 | tf_op jit(solution)/shard_map/all_gather | solution.py:43
  288.7 16.5 %fusion.6 = bf16[512,2048]{1,0:T(8,128)(2,1)} fusion(bf16[2048,4096]{1,0:T(8,128)(2,1)} %all-gather.12.cloned.1.call-done, bf16[512,2048]{1,0:T(8,128)(2,1)} %bitcast.180), kind=kOutput, calls=%fused_computation.8 | convolution fusion | flops 8594128896 | bytes 20971520 | tf_op jit(solution)/shard_map/dot_general | solution.py:194
  305.2 29.9 %all_to_all.16 = bf16[4,128,2048]{2,1,0:T(8,128)(2,1)S(1)} all-to-all(bf16[4,128,2048]{2,1,0:T(8,128)(2,1)} %bitcast.181), channel_id=1, replica_groups=mesh['grp'=2,'sp_0'=16,'sp_1'=2,'tp'=4] {'tp'}, dimensions={0} | all-to-all | bytes 4194304 | tf_op jit(solution)/shard_map/all_to_all | solution.py:58
  335.0 0.4 convert_reduce_fusion
  335.4 0.9 fusion.24
  (46 shorter events, 1.0 us)
Async XLA Ops:
  6.5 175.5 %copy-start = (bf16[512,2048]{1,0:T(8,128)(2,1)S(1)}, bf16[512,2048]{1,0:T(8,128)(2,1)}, u32[]{:S(2)}) copy-start(bf16[512,2048]{1,0:T(8,128)(2,1)} %param.27) | copy-start | bytes 6291460
  6.6 99.0 %copy-start.3 = (bf16[512,256]{1,0:T(8,128)(2,1)S(1)}, bf16[512,256]{1,0:T(8,128)(2,1)}, u32[]{:S(2)}) copy-start(bf16[512,256]{1,0:T(8,128)(2,1)} %param.22) | copy-start | bytes 786436
  6.6 45.5 %copy-start.4 = (bf16[2048,64]{0,1:T(8,128)(2,1)S(1)}, bf16[2048,64]{0,1:T(8,128)(2,1)}, u32[]{:S(2)}) copy-start(bf16[2048,64]{0,1:T(8,128)(2,1)} %param.31) | copy-start | bytes 786436
  6.6 45.5 %copy-start.5 = (bf16[64,2048]{1,0:T(8,128)(2,1)S(1)}, bf16[64,2048]{1,0:T(8,128)(2,1)}, u32[]{:S(2)}) copy-start(bf16[64,2048]{1,0:T(8,128)(2,1)} %param.30) | copy-start | bytes 786436
  6.6 104.4 %all-gather.10.cloned.1.call-start = ((), (), s32[]{:S(2)}) async-start(), calls=%async_computation.4 | async-start | bytes 1114112 | tf_op jit(solution)/shard_map/all_gather | solution.py:25
  45.9 130.0 %all-gather.8.cloned.1.call-start = ((), (), s32[]{:S(2)}) async-start(), calls=%async_computation.3 | async-start | bytes 4456448 | tf_op jit(solution)/shard_map/all_gather | solution.py:25
  52.0 236.7 %all-gather.12.cloned.1.call-start = ((), (), s32[]{:S(2)}) async-start(), calls=%async_computation.5 | async-start | bytes 17301504 | tf_op jit(solution)/shard_map/all_gather | solution.py:43
  107.9 6.2 %copy-start.7 = (f32[256]{0:T(256)S(1)}, f32[256]{0:T(256)}, u32[]{:S(2)}) copy-start(f32[256]{0:T(256)} %param.26) | copy-start | bytes 3076
  111.0 3.2 copy-start.2
  114.1 61.7 %copy-start.9 = (bf16[512,256]{1,0:T(8,128)(2,1)S(1)}, bf16[512,256]{1,0:T(8,128)(2,1)}, u32[]{:S(2)}) copy-start(bf16[512,256]{1,0:T(8,128)(2,1)} %param.17) | copy-start | bytes 786436
  175.9 6.2 %copy-start.1 = (f32[512,2048]{1,0:T(8,128)S(1)}, f32[512,2048]{1,0:T(8,128)}, u32[]{:S(2)}) copy-start(f32[512,2048]{1,0:T(8,128)} %fusion.116) | copy-start | bytes 12582916
  175.9 6.2 %copy-start.8 = (f32[512]{0:T(512)S(1)}, f32[512]{0:T(512)}, u32[]{:S(2)}) copy-start(f32[512]{0:T(512)} %param.25) | copy-start | bytes 6148
  184.9 24.6 %copy-start.6 = (f32[2048]{0:T(1024)S(1)}, f32[2048]{0:T(1024)}, u32[]{:S(2)}) copy-start(f32[2048]{0:T(1024)} %param.29) | copy-start | bytes 24580
  184.9 21.1 %all-to-all-start = ((bf16[4,128,2048]{2,1,0:T(8,128)(2,1)}), bf16[4,128,2048]{2,1,0:T(8,128)(2,1)}, u32[]{:S(2)}, u32[]{:S(2)}) async-start(bf16[4,128,2048]{2,1,0:T(8,128)(2,1)} %bitcast.179), calls=%async_computation | async-start | bytes 4194304 | tf_op jit(solution)/shard_map/all_to_all | solution.py:58
Sparse Core Ops, SparseCore 0:
  46.0 52.9 all-gather.9
  100.8 74.9 all-gather.7
  177.7 110.9 all-gather.11
where the time goes:
time: 344 us; the launch traced here: 343 us
  waiting for transfers between devices  136 us (40%)
  blocking collectives  99.3 us (29%)
  between operations  39.6 us (12%)
  matrix products  39.3 us (11%)
  other arithmetic  12.7 us (4%)
  local copies, waits for them, and re-layouts  11.4 us (3%)
  starting transfers between devices  4.84 us (1%)
    all_gather x1, waiting for transfers between devices, rows_first(): result, at, done = (lax.all_gather(both, axis, axis=0, tiled=True), 0, [])  60.1 us
    all_gather x2, waiting for transfers between devices, entering(): lax.all_gather(part.astype(kind), axis)  58.9 us
    all_to_all x1, blocking collectives, summed_on_arrival(): lax.all_to_all(parts, axis, split_axis=0, concat_axis=0, tiled=True)  29.9 us
    unnamed x2, blocking collectives  26.6 us
    all_gather x2, blocking collectives, entering(): lax.all_gather(part.astype(kind), axis)  24.2 us
    all_to_all x1, blocking collectives, copy_for_each(): lax.all_to_all(jnp.broadcast_to(x[None], (length, *x.shape)), axis, 0, 0,...  18.6 us
    dot_general x1, matrix products, on_device(): jnp.dot(hidden, down_full, preferred_element_type=jnp.float32)  16.5 us
    all_to_all x1, waiting for transfers between devices, summed_on_arrival(): lax.all_to_all(parts, axis, split_axis=0, concat_axis=0, tiled=True)  16.5 us
  transfers between devices with their start and end apart: 4, of which 3 were waited for; matrix products, arithmetic and copies ran while one was open for 10% of the time, Pallas kernels for 0%

commit v1 on v0

--- a/solution.py
+++ b/solution.py
@@ -40,7 +40,13 @@
 def rows_first(arrays, axis, dims):
     turned = [jnp.moveaxis(a, dim, 0) for a, dim in zip(arrays, dims)]
     both = jnp.concatenate([t.reshape(len(t), -1) for t in turned], axis=1)
-    result, at, done = (lax.all_gather(both, axis, axis=0, tiled=True), 0, [])
+    result, at, done = (
+        jnp.concatenate(
+            lax.all_to_all(jnp.stack([both] * lax.axis_size(axis)), axis, 0, 0), axis=0
+        ),
+        0,
+        [],
+    )
     for t, dim in zip(turned, dims):
         slab = result[:, at : at + t[0].size].reshape(-1, *t.shape[1:])
         done.append(jnp.moveaxis(slab, 0, dim))

time: 344 us -> 1040 us (3.02)
  blocking collectives: 99.3 us -> 830 us
  waiting for transfers between devices: 136 us -> 90.5 us
    all_to_all x1, blocking collectives: 18.6 us -> 749 us  [rows_first(): lax.all_to_all(jnp.stack([both] * lax.axis_size(axis)), axis, 0, 0)]
    all_gather x1 -> x0, waiting for transfers between devices: 60.1 us -> none  [rows_first(): result, at, done = (lax.all_gather(both, axis, axis=0, tiled=True), 0, [])]
    all_to_all x0 -> x1, waiting for transfers between devices: none -> 15.3 us  [copy_for_each(): lax.all_to_all(jnp.broadcast_to(x[None], (length, *x.shape)), axis, 0, 0,...]
  transfers between devices with their start and end apart: 4 -> 4, of which waited for: 3 -> 3; matrix products, arithmetic and copies ran while one was open for 10% -> 2% of each run, Pallas kernels for 0% -> 0%
where the time goes in v1:
time: 1040 us; the launch traced here: 1030 us
  blocking collectives  830 us (80%)
  waiting for transfers between devices  90.5 us (9%)
  between operations  40.4 us (4%)
  matrix products  39.3 us (4%)
  local copies, waits for them, and re-layouts  14.7 us (1%)
    all_to_all x1, blocking collectives, rows_first(): lax.all_to_all(jnp.stack([both] * lax.axis_size(axis)), axis, 0, 0)  749 us
    all_gather x2, waiting for transfers between devices, entering(): lax.all_gather(part.astype(kind), axis)  58.9 us
    all_to_all x1, blocking collectives, summed_on_arrival(): lax.all_to_all(parts, axis, split_axis=0, concat_axis=0, tiled=True)  29.7 us
    unnamed x2, blocking collectives  27.2 us
    all_gather x2, blocking collectives, entering(): lax.all_gather(part.astype(kind), axis)  24.2 us
  transfers between devices with their start and end apart: 4, of which 3 were waited for; matrix products, arithmetic and copies ran while one was open for 2% of the time, Pallas kernels for 0%

profile of v1, /device:TPU:33, one launch (start us, length us, event | category | flops | bytes accessed | tf_op | source)
XLA Modules:
  0.0 1033.9 jit_solution(7052849535006086324)
XLA Ops:
  6.6 1.1 reduce-window.16
  7.8 0.2 slice_reduce_fusion
  7.9 0.6 slice.382
  8.8 0.7 slice.383
  10.9 1.0 reduce-window.14
  11.9 0.2 slice_reduce_fusion.1
  12.1 0.6 slice.362
  12.9 0.6 slice.363
  14.8 1.3 dynamic-slice
  16.0 0.7 dynamic-update-slice
  16.7 0.7 dynamic-update-slice.2
  17.4 1.4 convolution_convert_fusion.1
  18.7 22.0 %all-gather.3 = bf16[256,256]{1,0:T(8,128)(2,1)S(1)} all-gather(bf16[128,256]{1,0:T(8,128)(2,1)S(1)} %convolution_convert_fusion.1), channel_id=5, replica_groups=mesh['grp'=2,'sp_0'=16,'sp_1'=2,'tp'=4] {'sp_1'}, dimensions={0}, use_global_device_ids=true | all-gather | bytes 196608 | tf_op jit(solution)/shard_map/all_gather | solution.py:25
  40.8 2.5 all-reduce.5
  43.2 0.7 slice_convert_fusion.1
  44.5 1.3 fusion.248
  46.6 1.5 convolution_convert_fusion
  48.2 2.2 all-gather.1
  50.4 1.5 fusion.115
  52.0 1.3 dynamic-slice.1
  53.3 0.7 fusion.317
  54.0 1.4 dynamic-update-slice.1
  55.4 1.4 dynamic-update-slice.3
  56.8 24.8 %all-reduce.4 = (bf16[16]{0:T(256)(128)(2,1)S(1)}, bf16[16]{0:T(256)(128)(2,1)S(1)}) all-reduce(bf16[16]{0:T(256)(128)(2,1)S(1)} %dynamic-update-slice.1, bf16[16]{0:T(256)(128)(2,1)S(1)} %dynamic-update-slice.3), channel_id=2, replica_groups=mesh['grp'=2,'sp_0'=16,'sp_1'=2,'tp'=4] {'sp_0'}, use_global_device_ids=true, to_apply=%add.1 | all-reduce | flops 32 | bytes 128
  82.8 0.7 fusion.316
  93.7 0.7 fusion.315
  105.9 2.3 fusion.18
  108.1 2.9 convolution_bitcast_fusion.1
  111.1 3.0 fusion.319
  114.3 2.8 fusion.116
  117.1 58.9 %all-gather.7.cloned.1.call-done = bf16[16,1,256,512]{3,2,1,0:T(8,128)(2,1)} async-done(((bf16[1,1,256,512]{3,2,1,0:T(8,128)(2,1)}), bf16[16,1,256,512]{3,2,1,0:T(8,128)(2,1)}) %all-gather.7.cloned.1.call-update) | async-done | bytes 4194320 | tf_op jit(solution)/shard_map/all_gather | solution.py:25
  175.9 6.0 fusion.320
  182.0 0.2 multiply_reduce_fusion
  182.2 2.8 add_convert_fusion
  185.0 4.1 all-to-all-start
  189.2 16.2 %all-to-all-done = bf16[4,128,2048]{2,1,0:T(8,128)(2,1)S(1)} async-done(((bf16[4,128,2048]{2,1,0:T(8,128)(2,1)}), bf16[4,128,2048]{2,1,0:T(8,128)(2,1)S(1)}, u32[]{:S(2)}, u32[]{:S(2)}) %all-to-all-start) | async-done | bytes 2097184 | tf_op jit(solution)/shard_map/all_to_all | solution.py:64
  205.4 0.4 convert_reduce_fusion.1
  205.7 1.3 fusion.21
  207.1 0.2 fusion.23
  207.3 1.6 broadcast_in_dim.16
  208.9 4.5 all-to-all-start.1
  213.5 15.3 %all-to-all-done.1 = bf16[4,128,2048]{2,1,0:T(8,128)(2,1)} async-done(((bf16[4,128,2048]{2,1,0:T(8,128)(2,1)}), bf16[4,128,2048]{2,1,0:T(8,128)(2,1)}, u32[]{:S(2)}, u32[]{:S(2)}) %all-to-all-start.1) | async-done | bytes 2097184 | tf_op jit(solution)/shard_map/all_to_all | solution.py:76
  228.8 1.9 stack.2
  230.7 748.8 %all_to_all.20 = bf16[32,64,4096]{2,1,0:T(8,128)(2,1)} all-to-all(bf16[32,64,4096]{2,1,0:T(8,128)(2,1)S(1)} %stack.2), channel_id=1, replica_groups=mesh['grp'=2,'sp_0'=16,'sp_1'=2,'tp'=4] {'sp_0','sp_1'}, dimensions={0} | all-to-all | bytes 33554432 | tf_op jit(solution)/shard_map/all_to_all | solution.py:45
  979.6 16.5 %fusion.6 = bf16[512,2048]{1,0:T(8,128)(2,1)} fusion(bf16[2048,4096]{1,0:T(8,128)(2,1)} %bitcast.180, bf16[512,2048]{1,0:T(8,128)(2,1)} %bitcast.75), kind=kOutput, calls=%fused_computation.8 | convolution fusion | flops 8594128896 | bytes 20971520 | tf_op jit(solution)/shard_map/dot_general | solution.py:200
  996.0 29.7 %all_to_all.21 = bf16[4,128,2048]{2,1,0:T(8,128)(2,1)S(1)} all-to-all(bf16[4,128,2048]{2,1,0:T(8,128)(2,1)} %bitcast.182), channel_id=1, replica_groups=mesh['grp'=2,'sp_0'=16,'sp_1'=2,'tp'=4] {'tp'}, dimensions={0} | all-to-all | bytes 4194304 | tf_op jit(solution)/shard_map/all_to_all | solution.py:64
  1025.7 0.4 convert_reduce_fusion
  1026.1 0.9 fusion.24
  (52 shorter events, 1.1 us)
Async XLA Ops:
  6.5 175.6 %copy-start = (bf16[512,2048]{1,0:T(8,128)(2,1)S(1)}, bf16[512,2048]{1,0:T(8,128)(2,1)}, u32[]{:S(2)}) copy-start(bf16[512,2048]{1,0:T(8,128)(2,1)} %param.27) | copy-start | bytes 6291460
  6.6 99.3 %copy-start.4 = (bf16[512,256]{1,0:T(8,128)(2,1)S(1)}, bf16[512,256]{1,0:T(8,128)(2,1)}, u32[]{:S(2)}) copy-start(bf16[512,256]{1,0:T(8,128)(2,1)} %param.22) | copy-start | bytes 786436
  6.6 99.3 %copy-start.7 = (bf16[512,128]{1,0:T(8,128)(2,1)S(1)}, bf16[512,128]{1,0:T(8,128)(2,1)}, u32[]{:S(2)}) copy-start(bf16[512,128]{1,0:T(8,128)(2,1)} %param.21) | copy-start | bytes 393220
  6.6 101.6 %copy-start.11 = (bf16[512,256]{1,0:T(8,128)(2,1)S(1)}, bf16[512,256]{1,0:T(8,128)(2,1)}, u32[]{:S(2)}) copy-start(bf16[512,256]{1,0:T(8,128)(2,1)} %param.18) | copy-start | bytes 786436
  6.6 104.5 %all-gather.9.cloned.1.call-start = ((), (), s32[]{:S(2)}) async-start(), calls=%async_computation.5 | async-start | bytes 1114112 | tf_op jit(solution)/shard_map/all_gather | solution.py:25
  45.8 130.1 %all-gather.7.cloned.1.call-start = ((), (), s32[]{:S(2)}) async-start(), calls=%async_computation.4 | async-start | bytes 4456448 | tf_op jit(solution)/shard_map/all_gather | solution.py:25
  108.1 6.1 copy-start.9
  111.1 3.2 copy-start.3
  114.2 61.7 %copy-start.12 = (bf16[512,256]{1,0:T(8,128)(2,1)S(1)}, bf16[512,256]{1,0:T(8,128)(2,1)}, u32[]{:S(2)}) copy-start(bf16[512,256]{1,0:T(8,128)(2,1)} %param.17) | copy-start | bytes 786436
  175.9 6.2 copy-start.2
  175.9 6.2 copy-start.10
  185.0 22.0 %copy-start.8 = (f32[2048]{0:T(1024)S(1)}, f32[2048]{0:T(1024)}, u32[]{:S(2)}) copy-start(f32[2048]{0:T(1024)} %param.29) | copy-start | bytes 24580
  185.0 20.3 %all-to-all-start = ((bf16[4,128,2048]{2,1,0:T(8,128)(2,1)}), bf16[4,128,2048]{2,1,0:T(8,128)(2,1)S(1)}, u32[]{:S(2)}, u32[]{:S(2)}) async-start(bf16[4,128,2048]{2,1,0:T(8,128)(2,1)} %bitcast.181), calls=%async_computation | async-start | bytes 4194304 | tf_op jit(solution)/shard_map/all_to_all | solution.py:64
  207.0 6.4 copy-start.5
  207.0 6.4 copy-start.6
  208.9 19.9 %all-to-all-start.1 = ((bf16[4,128,2048]{2,1,0:T(8,128)(2,1)}), bf16[4,128,2048]{2,1,0:T(8,128)(2,1)}, u32[]{:S(2)}, u32[]{:S(2)}) async-start(bf16[4,128,2048]{2,1,0:T(8,128)(2,1)} %broadcast_in_dim.16), calls=%async_computation.1 | async-start | bytes 4194304 | tf_op jit(solution)/shard_map/all_to_all | solution.py:76
  996.0 31.0 %copy-start.1 = (bf16[512,2048]{1,0:T(8,128)(2,1)S(1)}, bf16[512,2048]{1,0:T(8,128)(2,1)}, u32[]{:S(2)}) copy-start(bf16[512,2048]{1,0:T(8,128)(2,1)} %param.27) | copy-start | bytes 6291460
Sparse Core Ops, SparseCore 0:
  45.9 53.1 all-gather.8
  100.9 74.9 all-gather.6
